TPU v7x, 512 devices: a 8x2x16 block of a 8x16x16 slice. The times are simulated.
512 devices in a mesh: grp: 2 (over y), kv: 16 (over z), tp: 16 (over x, core).
Axes of the slice: x: 8, y: 2, z: 16, core: 2. Of those that a mesh axis runs over, the one named last changes fastest.
The devices are a block of a 8x16x16 slice.
Arguments:
- tokens: bfloat16 [256, 4096], P('grp', ('kv', 'tp')), parts along dimension 0, may hold values from -8 to 8
- norm_gain: bfloat16 [4096], P('kv'), may hold values from 0.099609375 to 1.8984375
- w_query: bfloat16 [4096, 1024], P('kv', 'tp'), may hold values from -0.09375 to 0.09375
- w_key: bfloat16 [4096, 1024], P('kv', 'tp'), may hold values from -0.09375 to 0.09375
- w_value: bfloat16 [4096, 2048], P('kv', 'tp'), may hold values from -0.09375 to 0.09375
- w_ogate: bfloat16 [4096, 2048], P('kv', 'tp'), may hold values from -0.09375 to 0.09375
- w_igate: bfloat16 [4096, 16], P('kv', 'tp'), may hold values from -0.09375 to 0.09375
- w_fgate: bfloat16 [4096, 16], P('kv', 'tp'), may hold values from -0.09375 to 0.09375
- igate_bias: float32 [16], P('tp'), may hold values from -1 to 1
- fgate_bias: float32 [16], P('tp'), may hold values from -1 to 4
- state_c: float32 [256, 16, 64, 128], P(('grp', 'kv'), 'tp'), parts along dimension 0, may hold values from -1.5 to 1.5
- state_n: float32 [256, 16, 64], P(('grp', 'kv'), 'tp'), parts along dimension 0, may hold values from -1.5 to 1.5
- state_m: float32 [256, 16], P(('grp', 'kv'), 'tp'), parts along dimension 0, may hold values from -3 to 1
- head_gain: bfloat16 [16, 128], P('tp'), may hold values from 0.099609375 to 1.8984375
- w_out: bfloat16 [2048, 4096], P('tp', 'kv'), may hold values from -0.125 to 0.125
- ffn_gain: bfloat16 [4096], P('kv'), may hold values from 0.099609375 to 1.8984375
- w_gate: bfloat16 [4096, 11008], P('kv', 'tp'), may hold values from -0.09375 to 0.09375
- w_up: bfloat16 [4096, 11008], P('kv', 'tp'), may hold values from -0.09375 to 0.09375
- w_down: bfloat16 [11008, 4096], P('tp', 'kv'), may hold values from -0.0546875 to 0.0546875
Outputs:
- out_tokens: bfloat16 [256, 4096], P('grp', ('kv', 'tp')), parts along dimension 0
- new_c: float32 [256, 16, 64, 128], P(('grp', 'kv'), 'tp'), parts along dimension 0
- new_n: float32 [256, 16, 64], P(('grp', 'kv'), 'tp'), parts along dimension 0
- new_m: float32 [256, 16], P(('grp', 'kv'), 'tp'), parts along dimension 0
There are 2 independent parts, one for each index of `grp`. A program takes and returns all parts, laid end to end along the dimension named above; an argument that names none is the same for every part. Nothing has to cross between parts.
All inputs are finite; a program needn't handle non-finite values.
Results may differ from a plain program's by a relative error of at most 0.017.
Values may be sent and summed in bfloat16 or wider, within the bound.
No kernel may reach another device: no remote copies, remote signals or barrier semaphores. Data moves between devices by JAX's collectives and lax.ppermute only.
A program may use at most 64 MiB of HBM per device.

v0:
```python
import math
import jax
import jax.numpy as jnp
from jax import lax
from jax.sharding import PartitionSpec as P

D = 4096
DK = 64
DV = 128
norm_eps = 1e-06
igate_cap = 1.5


def split_up(value, dim, count):
    before, after = (value.shape[:dim], value.shape[dim + 1 :])
    return jnp.moveaxis(value.reshape(*before, count, -1, *after), dim, 0)


def summed_on_arrival(value, axis, dim):
    blocks = split_up(value, dim, lax.axis_size(axis))
    arrived = lax.all_to_all(blocks, axis, split_axis=0, concat_axis=0, tiled=True)
    return arrived.sum(axis=0)


def side_by_side(arrays, axis, dim, along):
    columns = [a.reshape(*a.shape[:along], -1) for a in arrays]
    both = jnp.concatenate(columns, axis=along)
    out, at, finished = (summed_on_arrival(both, axis, dim), 0, [])
    for a, column in zip(arrays, columns):
        section = out[..., at : at + column.shape[along]]
        finished.append(section.reshape(*section.shape[:along], *a.shape[along:]))
        at += column.shape[along]
    return tuple(finished)


def in_order(blocks, dim):
    lengths = list(blocks.shape[1:])
    lengths[dim] *= blocks.shape[0]
    return jnp.moveaxis(blocks, 0, dim).reshape(lengths)


def sent_to_all(value, axis):
    count = lax.axis_size(axis)
    return lax.all_to_all(
        jnp.broadcast_to(value[None], (count, *value.shape)), axis, 0, 0, tiled=True
    )


def gathered_copies(value, axis, dim):
    return in_order(sent_to_all(value, axis), dim)


def sum_at_owner(value, axis, dim):
    blocks = split_up(value, dim, lax.axis_size(axis))
    arrived = lax.all_to_all(blocks, axis, split_axis=0, concat_axis=0, tiled=True)
    return arrived.astype(jnp.float32).sum(axis=0)


def side_by_side_2(arrays, axis, dim, along):
    widths = [math.prod(a.shape[along:]) for a in arrays]
    both = jnp.concatenate(
        [a.reshape(*a.shape[:along], w) for a, w in zip(arrays, widths)], axis=along
    )
    out = sum_at_owner(both, axis, dim)
    blocks = jnp.split(out, [sum(widths[:k]) for k in range(1, len(widths))], axis=along)
    return tuple((b.reshape(*out.shape[:along], *a.shape[along:]) for a, b in zip(arrays, blocks)))


def cell_update(query, key_vec, value_vec, igate, fgate, state_c, state_n, state_m):
    carried = jax.nn.log_sigmoid(fgate) + state_m
    new_m = jnp.maximum(carried, igate)
    keep_weight = jnp.exp(carried - new_m)
    write_weight = jnp.exp(igate - new_m)
    new_c = (
        keep_weight[..., None, None] * state_c
        + write_weight[..., None, None] * key_vec[..., :, None] * value_vec[..., None, :]
    )
    new_n = keep_weight[..., None] * state_n + write_weight[..., None] * key_vec
    numerator = jnp.einsum("bhd,bhde->bhe", query, new_c, precision=lax.Precision.HIGHEST)
    denominator = jnp.sum(query * new_n, axis=-1)
    head_out = numerator / jnp.maximum(jnp.abs(denominator), jnp.exp(-new_m))[..., None]
    return (new_c, new_n, new_m, head_out)


def body(
    tokens,
    norm_gain,
    w_query,
    w_key,
    w_value,
    w_ogate,
    w_igate,
    w_fgate,
    igate_bias,
    fgate_bias,
    state_c,
    state_n,
    state_m,
    head_gain,
    w_out,
    ffn_gain,
    w_gate,
    w_up,
    w_down,
):
    seq_rows = state_c.shape[0]
    heads_here = state_c.shape[1]
    token_cols = lax.all_gather(tokens, "tp", axis=1, tiled=True)
    token_vals = token_cols.astype(jnp.float32)
    normed = (token_vals * norm_gain.astype(jnp.float32)).astype(jnp.bfloat16)
    squares = jnp.sum(token_vals * token_vals, axis=1)
    part_query = jnp.dot(normed, w_query, preferred_element_type=jnp.float32)
    part_key = jnp.dot(normed, w_key, preferred_element_type=jnp.float32)
    part_value = jnp.dot(normed, w_value, preferred_element_type=jnp.float32)
    part_ogate = jnp.dot(normed, w_ogate, preferred_element_type=jnp.float32)
    part_igate = jnp.dot(normed, w_igate, preferred_element_type=jnp.float32)
    part_fgate = jnp.dot(normed, w_fgate, preferred_element_type=jnp.float32)
    sum_query, sum_key, sum_value, sum_ogate, sum_igate, sum_fgate, sum_squares = side_by_side(
        (part_query, part_key, part_value, part_ogate, part_igate, part_fgate, squares), "kv", 0, 1
    )
    row_scale = lax.rsqrt(sum_squares / D + norm_eps)[:, None]
    query = (row_scale * sum_query).reshape(seq_rows, heads_here, DK)
    key_vec = (row_scale * sum_key).reshape(seq_rows, heads_here, DK) * DK ** (-0.5)
    value_vec = (row_scale * sum_value).reshape(seq_rows, heads_here, DV)
    ogate = (row_scale * sum_ogate).reshape(seq_rows, heads_here, DV)
    igate = igate_cap * jnp.tanh((row_scale * sum_igate + igate_bias) / igate_cap)
    fgate = row_scale * sum_fgate + fgate_bias
    new_c, new_n, new_m, head_out = cell_update(
        query, key_vec, value_vec, igate, fgate, state_c, state_n, state_m
    )
    merged = (
        (head_out * head_gain.astype(jnp.float32) * jax.nn.sigmoid(ogate))
        .reshape(seq_rows, heads_here * DV)
        .astype(jnp.bfloat16)
    )
    attn_part = jnp.dot(gathered_copies(merged, "kv", 0), w_out, preferred_element_type=jnp.float32)
    attn_out = sum_at_owner(attn_part.astype(jnp.bfloat16), "tp", 1)
    middle = (tokens.astype(jnp.float32) + attn_out).astype(jnp.bfloat16)
    middle_cols = lax.all_gather(middle, "tp", axis=1, tiled=True)
    middle_vals = middle_cols.astype(jnp.float32)
    normed_two = (middle_vals * ffn_gain.astype(jnp.float32)).astype(jnp.bfloat16)
    squares_two = jnp.sum(middle_vals * middle_vals, axis=1)
    gate_part = jnp.dot(normed_two, w_gate, preferred_element_type=jnp.float32)
    up_part = jnp.dot(normed_two, w_up, preferred_element_type=jnp.float32)
    gate_sum, up_sum, total_two = side_by_side_2(
        (
            gate_part.astype(jnp.bfloat16),
            up_part.astype(jnp.bfloat16),
            squares_two.astype(jnp.bfloat16),
        ),
        "kv",
        0,
        1,
    )
    ffn_scale = lax.rsqrt(total_two / D + norm_eps)[:, None]
    hidden = (jax.nn.silu(ffn_scale * gate_sum) * (ffn_scale * up_sum)).astype(jnp.bfloat16)
    down_part = jnp.dot(
        gathered_copies(hidden, "kv", 0), w_down, preferred_element_type=jnp.float32
    )
    down_out = sum_at_owner(down_part.astype(jnp.bfloat16), "tp", 1)
    out_tokens = (middle.astype(jnp.float32) + down_out).astype(jnp.bfloat16)
    return (out_tokens, new_c, new_n, new_m)


def solution(mesh):
    placed = (
        P("grp", ("kv", "tp")),
        P("kv"),
        P("kv", "tp"),
        P("kv", "tp"),
        P("kv", "tp"),
        P("kv", "tp"),
        P("kv", "tp"),
        P("kv", "tp"),
        P("tp"),
        P("tp"),
        P(("grp", "kv"), "tp", None, None),
        P(("grp", "kv"), "tp", None),
        P(("grp", "kv"), "tp"),
        P("tp", None),
        P("tp", "kv"),
        P("kv"),
        P("kv", "tp"),
        P("kv", "tp"),
        P("tp", "kv"),
    )
    return jax.shard_map(
        body,
        mesh=mesh,
        in_specs=placed,
        out_specs=(
            P("grp", ("kv", "tp")),
            P(("grp", "kv"), "tp", None, None),
            P(("grp", "kv"), "tp", None),
            P(("grp", "kv"), "tp"),
        ),
        check_vma=False,
    )
```

profile of v0, /device:TPU:65, one launch (start us, length us, event | category | flops | bytes accessed | tf_op | source)
XLA Modules:
  0.0 202.4 jit_solution(7340011110046809596)
XLA Ops:
  0.6 0.7 convert_element_type.76
  1.4 55.9 %all_gather.6 = bf16[128,256]{0,1:T(8,128)(2,1)S(1)} all-gather(bf16[128,16]{0,1:T(8,128)(2,1)} %param.19), channel_id=1, replica_groups=mesh['grp'=2,'kv'=16,'tp'=16] {'tp'}, dimensions={1}, use_global_device_ids=true | all-gather | bytes 69632 | tf_op jit(solution)/shard_map/all_gather | solution.py:108
  57.3 0.1 copy.69
  57.4 0.1 fusion.4
  57.5 0.2 concatenate.31
  57.7 0.6 copy-done.8
  58.3 0.1 convolution_bitcast_fusion.4
  58.4 0.7 copy-done.5
  59.1 0.1 convolution_bitcast_fusion.3
  59.3 0.7 copy-done.6
  60.0 0.1 convolution_bitcast_fusion.2
  60.1 0.5 copy-done.12
  60.6 0.1 convolution_bitcast_fusion.1
  60.8 0.5 copy-done.13
  61.3 0.1 convolution_bitcast_fusion
  61.5 0.6 copy-done.9
  62.1 0.1 convolution_bitcast_fusion.5
  62.2 0.9 concatenate.27
  63.1 7.2 %all-to-all-start = ((f32[16,8,387]{2,1,0:T(8,128)}), f32[16,8,387]{2,1,0:T(8,128)S(1)}, u32[]{:S(2)}, u32[]{:S(2)}) async-start(f32[16,8,387]{2,1,0:T(8,128)} %concatenate.27), calls=%async_computation | async-start | bytes 524288 | tf_op jit(solution)/shard_map/all_to_all | solution.py:21
  71.7 12.5 %all-to-all-done = f32[16,8,387]{2,1,0:T(8,128)S(1)} async-done(((f32[16,8,387]{2,1,0:T(8,128)}), f32[16,8,387]{2,1,0:T(8,128)S(1)}, u32[]{:S(2)}, u32[]{:S(2)}) %all-to-all-start) | async-done | bytes 198176 | tf_op jit(solution)/shard_map/all_to_all | solution.py:21
  84.3 0.3 multiply_reduce_fusion
  84.6 0.7 copy-done.11
  85.3 0.8 fusion.39
  86.2 0.1 maximum_reduce_fusion
  86.3 0.1 multiply_add_fusion
  86.5 0.3 fusion
  86.9 21.4 %all_to_all.30 = bf16[16,8,128]{2,1,0:T(8,128)(2,1)S(1)} all-to-all(bf16[16,8,128]{2,1,0:T(8,128)(2,1)S(1)} %broadcast_in_dim.4), channel_id=1, replica_groups=mesh['grp'=2,'kv'=16,'tp'=16] {'kv'}, dimensions={0} | all-to-all | bytes 65536 | tf_op jit(solution)/shard_map/all_to_all | solution.py:44
  108.3 0.1 convolution_convert_fusion.3
  108.4 0.7 copy.78
  109.1 6.3 %all-to-all-start.2 = ((bf16[16,128,16]{1,2,0:T(8,128)(2,1)}), bf16[16,128,16]{1,2,0:T(8,128)(2,1)S(1)}, u32[]{:S(2)}, u32[]{:S(2)}) async-start(bf16[16,128,16]{1,2,0:T(8,128)(2,1)} %bitcast.23), calls=%async_computation.2 | async-start | bytes 131072 | tf_op jit(solution)/shard_map/all_to_all | solution.py:55
  115.5 7.7 %all-to-all-done.2 = bf16[16,128,16]{1,2,0:T(8,128)(2,1)S(1)} async-done(((bf16[16,128,16]{1,2,0:T(8,128)(2,1)}), bf16[16,128,16]{1,2,0:T(8,128)(2,1)S(1)}, u32[]{:S(2)}, u32[]{:S(2)}) %all-to-all-start.2) | async-done | bytes 65568 | tf_op jit(solution)/shard_map/all_to_all | solution.py:55
  123.3 15.0 %all_gather.7 = bf16[128,256]{0,1:T(8,128)(2,1)S(1)} all-gather(bf16[128,16]{0,1:T(8,128)(2,1)S(1)} %add_convert_fusion.1), channel_id=1, replica_groups=mesh['grp'=2,'kv'=16,'tp'=16] {'tp'}, dimensions={1}, use_global_device_ids=true | all-gather | bytes 69632 | tf_op jit(solution)/shard_map/all_gather | solution.py:139
  138.3 0.2 convert_element_type.95
  138.5 0.3 convolution_convert_fusion.1
  138.9 0.1 copy.79
  139.0 0.5 copy-done.2
  139.5 0.3 convolution_convert_fusion
  139.8 0.1 copy.80
  140.0 0.2 concatenate.30
  140.2 21.4 %all_to_all.31 = bf16[16,8,1377]{2,1,0:T(8,128)(2,1)S(1)} all-to-all(bf16[16,8,1377]{2,1,0:T(8,128)(2,1)S(1)} %concatenate.30), channel_id=1, replica_groups=mesh['grp'=2,'kv'=16,'tp'=16] {'kv'}, dimensions={0} | all-to-all | bytes 705024 | tf_op jit(solution)/shard_map/all_to_all | solution.py:55
  161.7 0.2 fusion.24
  162.0 22.1 %all_to_all.32 = bf16[16,8,688]{2,1,0:T(8,128)(2,1)S(1)} all-to-all(bf16[16,8,688]{2,1,0:T(8,128)(2,1)S(1)} %broadcast_in_dim.5), channel_id=1, replica_groups=mesh['grp'=2,'kv'=16,'tp'=16] {'kv'}, dimensions={0} | all-to-all | bytes 352256 | tf_op jit(solution)/shard_map/all_to_all | solution.py:44
  184.1 0.2 convolution_convert_fusion.2
  184.3 0.7 copy.82
  185.0 8.9 %all-to-all-start.5 = ((bf16[16,128,16]{1,2,0:T(8,128)(2,1)}), bf16[16,128,16]{1,2,0:T(8,128)(2,1)S(1)}, u32[]{:S(2)}, u32[]{:S(2)}) async-start(bf16[16,128,16]{1,2,0:T(8,128)(2,1)} %bitcast.28), calls=%async_computation.5 | async-start | bytes 131072 | tf_op jit(solution)/shard_map/all_to_all | solution.py:55
  194.0 0.6 copy.84
  194.6 7.2 %all-to-all-done.5 = bf16[16,128,16]{1,2,0:T(8,128)(2,1)S(1)} async-done(((bf16[16,128,16]{1,2,0:T(8,128)(2,1)}), bf16[16,128,16]{1,2,0:T(8,128)(2,1)S(1)}, u32[]{:S(2)}, u32[]{:S(2)}) %all-to-all-start.5) | async-done | bytes 65568 | tf_op jit(solution)/shard_map/all_to_all | solution.py:55
  201.8 0.6 add_convert_fusion
  (42 shorter events, 0.7 us)
Async XLA Ops:
  0.6 137.9 %copy-start = (bf16[256,688]{0,1:T(8,128)(2,1)S(1)}, bf16[256,688]{0,1:T(8,128)(2,1)}, u32[]{:S(2)}) copy-start(bf16[256,688]{0,1:T(8,128)(2,1)} %param.35) | copy-start | bytes 1056772
  57.5 0.8 copy-start.8
  58.3 0.8 copy-start.5
  59.1 0.8 copy-start.6
  60.0 0.7 copy-start.12
  60.6 0.7 copy-start.13
  61.3 0.8 copy-start.9
  63.1 8.6 %copy-start.14 = (f32[8,1]{0,1:T(1,128)S(1)}, f32[8,1]{0,1:T(1,128)}, u32[]{:S(2)}) copy-start(f32[8,1]{0,1:T(1,128)} %param.31) | copy-start | bytes 100
  63.1 8.7 %copy-start.15 = (bf16[1,128]{1,0:T(2,128)(2,1)S(1)}, bf16[1,128]{1,0:T(2,128)(2,1)}, u32[]{:S(2)}) copy-start(bf16[1,128]{1,0:T(2,128)(2,1)} %param.32) | copy-start | bytes 772
  63.1 21.2 %all-to-all-start = ((f32[16,8,387]{2,1,0:T(8,128)}), f32[16,8,387]{2,1,0:T(8,128)S(1)}, u32[]{:S(2)}, u32[]{:S(2)}) async-start(f32[16,8,387]{2,1,0:T(8,128)} %concatenate.27), calls=%async_computation | async-start | bytes 524288 | tf_op jit(solution)/shard_map/all_to_all | solution.py:21
  70.3 16.0 %copy-start.4 = (f32[8,1,64,128]{3,2,1,0:T(8,128)S(1)}, f32[8,1,64,128]{3,2,1,0:T(8,128)}, u32[]{:S(2)}) copy-start(f32[8,1,64,128]{3,2,1,0:T(8,128)} %param.29) | copy-start | bytes 786436
  84.6 0.7 copy-start.11
  86.4 22.0 %copy-start.1 = (f32[8,1,64,128]{3,2,1,0:T(8,128)}, f32[8,1,64,128]{3,2,1,0:T(8,128)S(1)}, u32[]{:S(2)}) copy-start(f32[8,1,64,128]{3,2,1,0:T(8,128)S(1)} %multiply_add_fusion) | copy-start | bytes 786436
  86.8 21.5 %copy-start.7 = (bf16[128,256]{1,0:T(8,128)(2,1)S(1)}, bf16[128,256]{1,0:T(8,128)(2,1)}, u32[]{:S(2)}) copy-start(bf16[128,256]{1,0:T(8,128)(2,1)} %param.33) | copy-start | bytes 196612
  109.1 6.3 %copy-start.16 = (bf16[256]{0:T(256)(128)(2,1)S(1)}, bf16[256]{0:T(256)(128)(2,1)}, u32[]{:S(2)}) copy-start(bf16[256]{0:T(256)(128)(2,1)} %param.34) | copy-start | bytes 1540
  109.1 14.1 %all-to-all-start.2 = ((bf16[16,128,16]{1,2,0:T(8,128)(2,1)}), bf16[16,128,16]{1,2,0:T(8,128)(2,1)S(1)}, u32[]{:S(2)}, u32[]{:S(2)}) async-start(bf16[16,128,16]{1,2,0:T(8,128)(2,1)} %bitcast.23), calls=%async_computation.2 | async-start | bytes 131072 | tf_op jit(solution)/shard_map/all_to_all | solution.py:55
  115.5 7.8 %copy-start.10 = (bf16[128,16]{0,1:T(8,128)(2,1)S(1)}, bf16[128,16]{0,1:T(8,128)(2,1)}, u32[]{:S(2)}) copy-start(bf16[128,16]{0,1:T(8,128)(2,1)} %param.19) | copy-start | bytes 12292
  138.5 1.0 copy-start.2
  161.7 22.4 %copy-start.3 = (bf16[688,256]{1,0:T(8,128)(2,1)S(1)}, bf16[688,256]{1,0:T(8,128)(2,1)}, u32[]{:S(2)}) copy-start(bf16[688,256]{1,0:T(8,128)(2,1)} %param.37) | copy-start | bytes 1056772
  185.0 16.7 %all-to-all-start.5 = ((bf16[16,128,16]{1,2,0:T(8,128)(2,1)}), bf16[16,128,16]{1,2,0:T(8,128)(2,1)S(1)}, u32[]{:S(2)}, u32[]{:S(2)}) async-start(bf16[16,128,16]{1,2,0:T(8,128)(2,1)} %bitcast.28), calls=%async_computation.5 | async-start | bytes 131072 | tf_op jit(solution)/shard_map/all_to_all | solution.py:55
where the time goes:
time: 203 us; the launch traced here: 202 us
  blocking collectives  136 us (67%)
  waiting for transfers between devices  27.4 us (13%)
  starting transfers between devices  22.5 us (11%)
  local copies, waits for them, and re-layouts  9 us (4%)
  other arithmetic  3.32 us (2%)
  between operations  2.24 us (1%)
  matrix products  2.09 us (1%)
    all_gather x1, blocking collectives, body(): token_cols = lax.all_gather(tokens, 'tp', axis=1, tiled=True)  55.9 us
    all_to_all x2, blocking collectives, sent_to_all(): lax.all_to_all(jnp.broadcast_to(value[None], (count, *value.shape)), axis...  43.5 us
    all_to_all x1, blocking collectives, sum_at_owner(): lax.all_to_all(blocks, axis, split_axis=0, concat_axis=0, tiled=True)  21.4 us
    all_to_all x2, starting transfers between devices, sum_at_owner(): lax.all_to_all(blocks, axis, split_axis=0, concat_axis=0, tiled=True)  15.3 us
    all_gather x1, blocking collectives, body(): middle_cols = lax.all_gather(middle, 'tp', axis=1, tiled=True)  15 us
    all_to_all x2, waiting for transfers between devices, sum_at_owner(): lax.all_to_all(blocks, axis, split_axis=0, concat_axis=0, tiled=True)  14.9 us
    all_to_all x1, waiting for transfers between devices, summed_on_arrival(): lax.all_to_all(blocks, axis, split_axis=0, concat_axis=0, tiled=True)  12.5 us
    all_to_all x1, starting transfers between devices, summed_on_arrival(): lax.all_to_all(blocks, axis, split_axis=0, concat_axis=0, tiled=True)  7.23 us
  transfers between devices with their start and end apart: 3, of which 3 were waited for; matrix products, arithmetic and copies ran while one was open for 0% of the time, Pallas kernels for 0%

commit v1 on v0

--- a/solution.py
+++ b/solution.py
@@ -9,6 +9,14 @@
 DV = 128
 norm_eps = 1e-06
 igate_cap = 1.5
+
+
+def gather_by_exchange(array, axis, dim):
+    size = lax.axis_size(axis)
+    repeats = [size if d == dim else 1 for d in range(array.ndim)]
+    return lax.all_to_all(
+        jnp.tile(array, repeats), axis, split_axis=dim, concat_axis=dim, tiled=True
+    )
 
 
 def split_up(value, dim, count):
@@ -105,7 +113,7 @@
 ):
     seq_rows = state_c.shape[0]
     heads_here = state_c.shape[1]
-    token_cols = lax.all_gather(tokens, "tp", axis=1, tiled=True)
+    token_cols = gather_by_exchange(tokens, "tp", 1)
     token_vals = token_cols.astype(jnp.float32)
     normed = (token_vals * norm_gain.astype(jnp.float32)).astype(jnp.bfloat16)
     squares = jnp.sum(token_vals * token_vals, axis=1)

time: 203 us -> 202 us (level)
  blocking collectives: 136 us -> 79.8 us
  starting transfers between devices: 22.5 us -> 66.6 us
  waiting for transfers between devices: 27.4 us -> 35.5 us
  local copies, waits for them, and re-layouts: 9 us -> 12 us
    all_gather x1 -> x0, blocking collectives: 55.9 us -> none  [body(): token_cols = lax.all_gather(tokens, 'tp', axis=1, tiled=True)]
    all_to_all x0 -> x1, starting transfers between devices: none -> 44.9 us  [gather_by_exchange(): lax.all_to_all(jnp.tile(array, repeats), axis, split_axis=dim, concat_axi...]
    all_to_all x0 -> x1, waiting for transfers between devices: none -> 7.82 us  [gather_by_exchange(): lax.all_to_all(jnp.tile(array, repeats), axis, split_axis=dim, concat_axi...]
    unnamed x36 -> x38, local copies, waits for them, and re-layouts: 5.57 us -> 5.45 us
  transfers between devices with their start and end apart: 3 -> 4, of which waited for: 3 -> 4; matrix products, arithmetic and copies ran while one was open for 0% -> 0% of each run, Pallas kernels for 0% -> 0%
where the time goes in v1:
time: 202 us; the launch traced here: 201 us
  blocking collectives  79.8 us (40%)
  starting transfers between devices  66.6 us (33%)
  waiting for transfers between devices  35.5 us (18%)
  local copies, waits for them, and re-layouts  12 us (6%)
  other arithmetic  2.64 us (1%)
  between operations  2.23 us (1%)
  matrix products  2.09 us (1%)
    all_to_all x1, starting transfers between devices, gather_by_exchange(): lax.all_to_all(jnp.tile(array, repeats), axis, split_axis=dim, concat_axi...  44.9 us
    all_to_all x2, blocking collectives, sent_to_all(): lax.all_to_all(jnp.broadcast_to(value[None], (count, *value.shape)), axis...  43.4 us
    all_to_all x1, blocking collectives, sum_at_owner(): lax.all_to_all(blocks, axis, split_axis=0, concat_axis=0, tiled=True)  21.4 us
    all_to_all x2, waiting for transfers between devices, sum_at_owner(): lax.all_to_all(blocks, axis, split_axis=0, concat_axis=0, tiled=True)  15.1 us
    all_gather x1, blocking collectives, body(): middle_cols = lax.all_gather(middle, 'tp', axis=1, tiled=True)  14.9 us
    all_to_all x2, starting transfers between devices, sum_at_owner(): lax.all_to_all(blocks, axis, split_axis=0, concat_axis=0, tiled=True)  14.3 us
    all_to_all x1, waiting for transfers between devices, summed_on_arrival(): lax.all_to_all(blocks, axis, split_axis=0, concat_axis=0, tiled=True)  12.6 us
    all_to_all x1, waiting for transfers between devices, gather_by_exchange(): lax.all_to_all(jnp.tile(array, repeats), axis, split_axis=dim, concat_axi...  7.82 us
  transfers between devices with their start and end apart: 4, of which 4 were waited for; matrix products, arithmetic and copies ran while one was open for 0% of the time, Pallas kernels for 0%

profile of v1, /device:TPU:65, one launch (start us, length us, event | category | flops | bytes accessed | tf_op | source)
XLA Modules:
  0.0 200.8 jit_solution(3735989059813873766)
XLA Ops:
  0.6 1.4 tile.2
  2.0 44.9 %all-to-all-start = ((bf16[128,16,16]{0,2,1:T(8,128)(2,1)}), bf16[128,16,16]{0,2,1:T(8,128)(2,1)S(1)}, u32[]{:S(2)}, u32[]{:S(2)}) async-start(bf16[128,16,16]{0,2,1:T(8,128)(2,1)} %tile.2), calls=%async_computation | async-start | bytes 131072 | tf_op jit(solution)/shard_map/all_to_all | solution.py:17
  47.0 7.8 %all-to-all-done = bf16[128,16,16]{0,2,1:T(8,128)(2,1)S(1)} async-done(((bf16[128,16,16]{0,2,1:T(8,128)(2,1)}), bf16[128,16,16]{0,2,1:T(8,128)(2,1)S(1)}, u32[]{:S(2)}, u32[]{:S(2)}) %all-to-all-start) | async-done | bytes 65568 | tf_op jit(solution)/shard_map/all_to_all | solution.py:17
  54.8 0.4 copy.65
  55.3 0.4 reshape.211
  55.7 0.7 copy-done.8
  56.5 0.1 fusion.10
  56.6 0.6 copy-done.9
  57.2 0.1 fusion.12
  57.3 0.7 copy-done.5
  58.1 0.1 fusion.5
  58.2 0.7 copy-done.6
  58.9 0.1 fusion.7
  59.2 0.4 copy.66
  59.6 0.5 dot_general.43
  60.1 0.2 copy-done.12
  60.4 0.6 copy-done.13
  61.1 0.2 concatenate.19
  61.3 0.8 concatenate.15
  62.1 7.4 %all-to-all-start.1 = ((f32[16,8,387]{2,1,0:T(8,128)}), f32[16,8,387]{2,1,0:T(8,128)S(1)}, u32[]{:S(2)}, u32[]{:S(2)}) async-start(f32[16,8,387]{2,1,0:T(8,128)} %concatenate.15), calls=%async_computation.1 | async-start | bytes 524288 | tf_op jit(solution)/shard_map/all_to_all | solution.py:29
  71.0 12.6 %all-to-all-done.1 = f32[16,8,387]{2,1,0:T(8,128)S(1)} async-done(((f32[16,8,387]{2,1,0:T(8,128)}), f32[16,8,387]{2,1,0:T(8,128)S(1)}, u32[]{:S(2)}, u32[]{:S(2)}) %all-to-all-start.1) | async-done | bytes 198176 | tf_op jit(solution)/shard_map/all_to_all | solution.py:29
  83.6 0.3 multiply_reduce_fusion.1
  83.9 0.7 copy-done.11
  84.6 0.8 fusion.37
  85.6 0.1 multiply_add_fusion
  85.7 0.3 fusion
  86.2 21.4 %all_to_all.36 = bf16[16,8,128]{2,1,0:T(8,128)(2,1)S(1)} all-to-all(bf16[16,8,128]{2,1,0:T(8,128)(2,1)S(1)} %broadcast_in_dim.4), channel_id=1, replica_groups=mesh['grp'=2,'kv'=16,'tp'=16] {'kv'}, dimensions={0} | all-to-all | bytes 65536 | tf_op jit(solution)/shard_map/all_to_all | solution.py:52
  107.5 0.1 convolution_convert_fusion.3
  107.7 0.7 copy.73
  108.4 5.4 %all-to-all-start.3 = ((bf16[16,128,16]{1,2,0:T(8,128)(2,1)}), bf16[16,128,16]{1,2,0:T(8,128)(2,1)S(1)}, u32[]{:S(2)}, u32[]{:S(2)}) async-start(bf16[16,128,16]{1,2,0:T(8,128)(2,1)} %bitcast.22), calls=%async_computation.3 | async-start | bytes 131072 | tf_op jit(solution)/shard_map/all_to_all | solution.py:63
  113.8 7.9 %all-to-all-done.3 = bf16[16,128,16]{1,2,0:T(8,128)(2,1)S(1)} async-done(((bf16[16,128,16]{1,2,0:T(8,128)(2,1)}), bf16[16,128,16]{1,2,0:T(8,128)(2,1)S(1)}, u32[]{:S(2)}, u32[]{:S(2)}) %all-to-all-start.3) | async-done | bytes 65568 | tf_op jit(solution)/shard_map/all_to_all | solution.py:63
  121.7 14.9 %all_gather.3 = bf16[128,256]{0,1:T(8,128)(2,1)S(1)} all-gather(bf16[128,16]{0,1:T(8,128)(2,1)S(1)} %add_convert_fusion.1), channel_id=1, replica_groups=mesh['grp'=2,'kv'=16,'tp'=16] {'tp'}, dimensions={1}, use_global_device_ids=true | all-gather | bytes 69632 | tf_op jit(solution)/shard_map/all_gather | solution.py:147
  136.7 0.3 convolution_convert_fusion.1
  137.1 0.1 copy.74
  137.2 0.5 copy-done.2
  137.7 0.3 convolution_convert_fusion
  138.0 0.1 copy.75
  138.2 0.2 convert_element_type.119
  138.4 0.2 concatenate.18
  138.6 21.4 %all_to_all.37 = bf16[16,8,1377]{2,1,0:T(8,128)(2,1)S(1)} all-to-all(bf16[16,8,1377]{2,1,0:T(8,128)(2,1)S(1)} %concatenate.18), channel_id=1, replica_groups=mesh['grp'=2,'kv'=16,'tp'=16] {'kv'}, dimensions={0} | all-to-all | bytes 705024 | tf_op jit(solution)/shard_map/all_to_all | solution.py:63
  160.1 0.2 fusion.22
  160.4 22.1 %all_to_all.38 = bf16[16,8,688]{2,1,0:T(8,128)(2,1)S(1)} all-to-all(bf16[16,8,688]{2,1,0:T(8,128)(2,1)S(1)} %broadcast_in_dim.5), channel_id=1, replica_groups=mesh['grp'=2,'kv'=16,'tp'=16] {'kv'}, dimensions={0} | all-to-all | bytes 352256 | tf_op jit(solution)/shard_map/all_to_all | solution.py:52
  182.5 0.2 convolution_convert_fusion.2
  182.8 0.7 copy.77
  183.5 9.0 %all-to-all-start.6 = ((bf16[16,128,16]{1,2,0:T(8,128)(2,1)}), bf16[16,128,16]{1,2,0:T(8,128)(2,1)S(1)}, u32[]{:S(2)}, u32[]{:S(2)}) async-start(bf16[16,128,16]{1,2,0:T(8,128)(2,1)} %bitcast.27), calls=%async_computation.6 | async-start | bytes 131072 | tf_op jit(solution)/shard_map/all_to_all | solution.py:63
  192.4 0.6 copy.79
  193.0 7.2 %all-to-all-done.6 = bf16[16,128,16]{1,2,0:T(8,128)(2,1)S(1)} async-done(((bf16[16,128,16]{1,2,0:T(8,128)(2,1)}), bf16[16,128,16]{1,2,0:T(8,128)(2,1)S(1)}, u32[]{:S(2)}, u32[]{:S(2)}) %all-to-all-start.6) | async-done | bytes 65568 | tf_op jit(solution)/shard_map/all_to_all | solution.py:63
  200.2 0.6 add_convert_fusion
  (51 shorter events, 1.3 us)
Async XLA Ops:
  0.6 136.1 %copy-start = (bf16[256,688]{0,1:T(8,128)(2,1)S(1)}, bf16[256,688]{0,1:T(8,128)(2,1)}, u32[]{:S(2)}) copy-start(bf16[256,688]{0,1:T(8,128)(2,1)} %param.35) | copy-start | bytes 1056772
  2.0 44.9 %copy-start.14 = (bf16[256]{0:T(256)(128)(2,1)S(1)}, bf16[256]{0:T(256)(128)(2,1)}, u32[]{:S(2)}) copy-start(bf16[256]{0:T(256)(128)(2,1)} %param.20) | copy-start | bytes 1540
  2.0 52.8 %all-to-all-start = ((bf16[128,16,16]{0,2,1:T(8,128)(2,1)}), bf16[128,16,16]{0,2,1:T(8,128)(2,1)S(1)}, u32[]{:S(2)}, u32[]{:S(2)}) async-start(bf16[128,16,16]{0,2,1:T(8,128)(2,1)} %tile.2), calls=%async_computation | async-start | bytes 131072 | tf_op jit(solution)/shard_map/all_to_all | solution.py:17
  55.7 0.8 copy-start.8
  56.5 0.8 copy-start.9
  57.2 0.8 copy-start.5
  58.1 0.8 copy-start.6
  59.6 0.7 copy-start.12
  60.3 0.7 copy-start.13
  62.1 7.4 %copy-start.15 = (f32[8,1]{0,1:T(1,128)S(1)}, f32[8,1]{0,1:T(1,128)}, u32[]{:S(2)}) copy-start(f32[8,1]{0,1:T(1,128)} %param.31) | copy-start | bytes 100
  62.1 8.8 %copy-start.16 = (bf16[1,128]{1,0:T(2,128)(2,1)S(1)}, bf16[1,128]{1,0:T(2,128)(2,1)}, u32[]{:S(2)}) copy-start(bf16[1,128]{1,0:T(2,128)(2,1)} %param.32) | copy-start | bytes 772
  62.1 21.4 %all-to-all-start.1 = ((f32[16,8,387]{2,1,0:T(8,128)}), f32[16,8,387]{2,1,0:T(8,128)S(1)}, u32[]{:S(2)}, u32[]{:S(2)}) async-start(f32[16,8,387]{2,1,0:T(8,128)} %concatenate.15), calls=%async_computation.1 | async-start | bytes 524288 | tf_op jit(solution)/shard_map/all_to_all | solution.py:29
  69.6 16.0 %copy-start.4 = (f32[8,1,64,128]{3,2,1,0:T(8,128)S(1)}, f32[8,1,64,128]{3,2,1,0:T(8,128)}, u32[]{:S(2)}) copy-start(f32[8,1,64,128]{3,2,1,0:T(8,128)} %param.29) | copy-start | bytes 786436
  83.9 0.7 copy-start.11
  85.7 21.9 %copy-start.1 = (f32[8,1,64,128]{3,2,1,0:T(8,128)}, f32[8,1,64,128]{3,2,1,0:T(8,128)S(1)}, u32[]{:S(2)}) copy-start(f32[8,1,64,128]{3,2,1,0:T(8,128)S(1)} %multiply_add_fusion) | copy-start | bytes 786436
  86.1 21.5 %copy-start.7 = (bf16[128,256]{1,0:T(8,128)(2,1)S(1)}, bf16[128,256]{1,0:T(8,128)(2,1)}, u32[]{:S(2)}) copy-start(bf16[128,256]{1,0:T(8,128)(2,1)} %param.33) | copy-start | bytes 196612
  108.4 5.4 %copy-start.17 = (bf16[256]{0:T(256)(128)(2,1)S(1)}, bf16[256]{0:T(256)(128)(2,1)}, u32[]{:S(2)}) copy-start(bf16[256]{0:T(256)(128)(2,1)} %param.34) | copy-start | bytes 1540
  108.4 13.3 %all-to-all-start.3 = ((bf16[16,128,16]{1,2,0:T(8,128)(2,1)}), bf16[16,128,16]{1,2,0:T(8,128)(2,1)S(1)}, u32[]{:S(2)}, u32[]{:S(2)}) async-start(bf16[16,128,16]{1,2,0:T(8,128)(2,1)} %bitcast.22), calls=%async_computation.3 | async-start | bytes 131072 | tf_op jit(solution)/shard_map/all_to_all | solution.py:63
  113.8 7.9 %copy-start.10 = (bf16[128,16]{0,1:T(8,128)(2,1)S(1)}, bf16[128,16]{0,1:T(8,128)(2,1)}, u32[]{:S(2)}) copy-start(bf16[128,16]{0,1:T(8,128)(2,1)} %param.19) | copy-start | bytes 12292
  136.7 1.0 copy-start.2
  160.1 22.4 %copy-start.3 = (bf16[688,256]{1,0:T(8,128)(2,1)S(1)}, bf16[688,256]{1,0:T(8,128)(2,1)}, u32[]{:S(2)}) copy-start(bf16[688,256]{1,0:T(8,128)(2,1)} %param.37) | copy-start | bytes 1056772
  183.5 16.7 %all-to-all-start.6 = ((bf16[16,128,16]{1,2,0:T(8,128)(2,1)}), bf16[16,128,16]{1,2,0:T(8,128)(2,1)S(1)}, u32[]{:S(2)}, u32[]{:S(2)}) async-start(bf16[16,128,16]{1,2,0:T(8,128)(2,1)} %bitcast.27), calls=%async_computation.6 | async-start | bytes 131072 | tf_op jit(solution)/shard_map/all_to_all | solution.py:63
